TPU v7x, 32 devices: a whole 2x2x4 slice. The times are simulated.
32 devices in a mesh: sp: 8 (over z, y), tp: 4 (over x, core).
Axes of the slice: x: 2, y: 2, z: 4, core: 2. Of those that a mesh axis runs over, the one named last changes fastest.
Arguments:
- inputs: bfloat16 [8192, 2048], P('sp'), may hold values from -6 to 6
- norm_gain: float32 [3, 2048], replicated, may hold values from 0.1 to 1.9
- query_weight: bfloat16 [3, 2048, 1024], P(None, 'sp', 'tp'), may hold values from -64 to 64
- key_weight: bfloat16 [3, 2048, 512], P(None, 'sp', 'tp'), may hold values from -4 to 4
- value_weight: bfloat16 [3, 2048, 512], P(None, 'sp', 'tp'), may hold values from -0.125 to 0.125
- output_weight: bfloat16 [3, 2048, 1024], P(None, 'sp', 'tp'), may hold values from -0.1875 to 0.1875
- sink_logit: float32 [3, 16], P(None, 'tp'), may hold values from 2 to 7
- final_gain: float32 [2048], replicated, may hold values from 0.1 to 1.9
Outputs:
- result: float32 [8192, 2048], P(('sp', 'tp'))
All inputs are finite; a program needn't handle non-finite values.
Results may differ from a plain program's by a relative error of at most 0.015.
Values may be sent and summed in bfloat16 or wider, within the bound.
A program may use at most 64 MiB of HBM per device.

v0:
```python
import jax
import jax.numpy as jnp
from jax import lax
from jax.sharding import PartitionSpec as P

D = 2048
HEAD_DIM = 64
WINDOW = 128
LAYERS = 3


EPS = 1e-06


def extended_2(block, sides, width):
    for axis, dim in sides:
        count = lax.axis_size(axis)
        forward = [(i, i + 1) for i in range(count - 1)]
        backward = [(target, source) for source, target in forward]
        low = lax.ppermute(
            lax.slice_in_dim(block, block.shape[dim] - width, None, axis=dim), axis, forward
        )
        high = lax.ppermute(lax.slice_in_dim(block, 0, width, axis=dim), axis, backward)
        block = jnp.concatenate([low, block, high], axis=dim)
    return block


def norm_rows(values, gain):
    wide_values = values.astype(jnp.float32)
    inv_root = lax.rsqrt(jnp.mean(wide_values * wide_values, axis=-1, keepdims=True) + EPS)
    return wide_values * inv_root * gain


def rotate(values, places):
    half_dim = values.shape[-1] // 2
    inverse = 10000.0 ** (-jnp.arange(half_dim).astype(jnp.float32) / half_dim)
    angles = places[:, None] * inverse[None, :]
    cosine_table = jnp.cos(angles)[:, None, :]
    sine_table = jnp.sin(angles)[:, None, :]
    front_half = values[..., :half_dim]
    back_half = values[..., half_dim:]
    return jnp.concatenate(
        [
            front_half * cosine_table - back_half * sine_table,
            back_half * cosine_table + front_half * sine_table,
        ],
        axis=-1,
    )


def attend(queries, key_rows, value_rows, sink_row, allowed):
    scores = jnp.einsum(
        "qkgd,skd->kgqs", queries, key_rows, preferred_element_type=jnp.float32
    ) * queries.shape[-1] ** (-0.5)
    scores = jnp.where(allowed[None, None], scores, -jnp.inf)
    sink_col = sink_row[:, :, None]
    largest = jnp.maximum(jnp.max(scores, axis=-1), sink_col)
    powers = jnp.exp(scores - largest[..., None])
    denominator = jnp.sum(powers, axis=-1) + jnp.exp(sink_col - largest)
    weights = (powers / denominator[..., None]).astype(jnp.bfloat16)
    blended = jnp.einsum("kgqs,skd->qkgd", weights, value_rows, preferred_element_type=jnp.float32)
    return blended.astype(jnp.bfloat16)


def shards(
    inputs, norm_gain, query_weight, key_weight, value_weight, output_weight, sink_logit, final_gain
):
    tokens = inputs.shape[0]
    local_heads = query_weight.shape[2] // HEAD_DIM
    local_groups = key_weight.shape[2] // HEAD_DIM
    per_group = local_heads // local_groups
    kv_cols = local_groups * HEAD_DIM
    offset = lax.axis_index("sp") * tokens
    seq_total = tokens * lax.axis_size("sp")
    query_pos = offset + jnp.arange(tokens, dtype=jnp.int32)
    places = query_pos.astype(jnp.float32)
    key_pos = offset - WINDOW + jnp.arange(tokens + 2 * WINDOW, dtype=jnp.int32)
    allowed = (
        (jnp.abs(key_pos[None, :] - query_pos[:, None]) <= WINDOW)
        & (key_pos[None, :] >= 0)
        & (key_pos[None, :] < seq_total)
    )
    whole_query, whole_key, whole_value, whole_out = (
        lax.all_gather(query_weight, "sp", axis=1, tiled=True),
        lax.all_gather(key_weight, "sp", axis=1, tiled=True),
        lax.all_gather(value_weight, "sp", axis=1, tiled=True),
        lax.all_gather(output_weight, "sp", axis=1, tiled=True),
    )
    current = inputs
    final_rows = inputs
    for layer in range(LAYERS):
        normed = norm_rows(current, norm_gain[layer]).astype(jnp.bfloat16)
        query_raw = jnp.dot(normed, whole_query[layer], preferred_element_type=jnp.float32)
        key_raw = jnp.dot(normed, whole_key[layer], preferred_element_type=jnp.float32)
        value_raw = jnp.dot(normed, whole_value[layer], preferred_element_type=jnp.float32)
        out_weight = whole_out[layer]
        queries = rotate(
            (query_raw * float(D) ** (-0.5)).reshape(tokens, local_heads, HEAD_DIM), places
        ).astype(jnp.bfloat16)
        key_rot = rotate(
            (key_raw * float(D) ** (-0.5)).reshape(tokens, local_groups, HEAD_DIM), places
        ).astype(jnp.bfloat16)
        packed = jnp.concatenate(
            [key_rot.reshape(tokens, kv_cols), value_raw.astype(jnp.bfloat16)], axis=1
        )
        extended = extended_2(packed, (("sp", 0),), WINDOW)
        key_rows = extended[:, :kv_cols].reshape(-1, local_groups, HEAD_DIM)
        value_all = extended[:, kv_cols:].reshape(-1, local_groups, HEAD_DIM)
        sink_row = sink_logit[layer].reshape(local_groups, per_group)
        attended = attend(
            queries.reshape(tokens, local_groups, per_group, HEAD_DIM),
            key_rows,
            value_all,
            sink_row,
            allowed,
        )
        attended = attended.reshape(tokens, local_heads * HEAD_DIM)

        def project():
            return lax.dot_general(
                attended, out_weight, (((1,), (1,)), ((), ())), preferred_element_type=jnp.float32
            )

        if layer < LAYERS - 1:
            share_rows = lax.psum_scatter(project(), "tp", scatter_dimension=0, tiled=True).astype(
                jnp.bfloat16
            )
            current = lax.all_gather(share_rows, "tp", axis=0, tiled=True)
        else:
            final_rows = lax.psum_scatter(
                project().astype(jnp.bfloat16), "tp", scatter_dimension=0, tiled=True
            )
    return norm_rows(final_rows, final_gain)


def solution(mesh):
    in_specs = (
        P("sp", None),
        P(),
        P(None, "sp", "tp"),
        P(None, "sp", "tp"),
        P(None, "sp", "tp"),
        P(None, "sp", "tp"),
        P(None, "tp"),
        P(),
    )
    out_specs = P(("sp", "tp"), None)
    return jax.shard_map(shards, mesh=mesh, in_specs=in_specs, out_specs=out_specs, check_vma=False)
```

profile of v0, /device:TPU:8, one launch (start us, length us, event | category | flops | bytes accessed | tf_op | source)
XLA Modules:
  0.0 579.0 jit_solution(9668719352871353835)
XLA Ops:
  6.5 0.7 all-gather.7.cloned.1.call-update
  7.3 0.7 all-gather.9.cloned.1.call-update
  8.1 0.7 all-gather.11.cloned.1.call-update
  8.8 0.5 all-gather.13.cloned.1.call-update
  9.4 1.0 fusion.54
  10.4 3.3 fusion.9
  13.8 3.0 fusion.11
  16.7 0.5 multiply_cosine_fusion
  17.3 2.3 fusion.19
  19.5 35.3 %all-gather.7.cloned.1.call-done = bf16[3,2048,128]{2,1,0:T(8,128)(2,1)} async-done(((bf16[3,256,128]{2,1,0:T(8,128)(2,1)}), bf16[3,2048,128]{2,1,0:T(8,128)(2,1)}) %all-gather.7.cloned.1.call-update) | async-done | bytes 1572880 | tf_op jit(solution)/shard_map/all_gather | solution.py:85
  54.9 3.8 convolution_multiply_fusion.5
  58.8 40.8 %all-gather.9.cloned.1.call-done = bf16[3,2048,128]{2,1,0:T(8,128)(2,1)} async-done(((bf16[3,256,128]{2,1,0:T(8,128)(2,1)}), bf16[3,2048,128]{2,1,0:T(8,128)(2,1)}) %all-gather.9.cloned.1.call-update) | async-done | bytes 1572880 | tf_op jit(solution)/shard_map/all_gather | solution.py:86
  99.7 3.8 convolution_convert_fusion.3
  103.5 2.5 collective-permute-start.1
  106.0 3.8 collective-permute-start
  110.0 4.4 collective-permute-done
  114.5 46.3 %all-gather.11.cloned.1.call-done = bf16[3,2048,256]{2,1,0:T(8,128)(2,1)} async-done(((bf16[3,256,256]{2,1,0:T(8,128)(2,1)}), bf16[3,2048,256]{2,1,0:T(8,128)(2,1)}) %all-gather.11.cloned.1.call-update) | async-done | bytes 3145744 | tf_op jit(solution)/shard_map/all_gather | solution.py:84
  160.9 3.8 convolution_multiply_fusion.2
  164.6 0.2 subtract_convert_fusion.2
  164.8 3.7 fusion.3
  168.6 4.7 fusion
  173.3 6.2 %fusion.24 = bf16[2,64,2,1024]{3,1,2,0:T(8,128)(2,1)S(1)} fusion(bf16[1280,2,64,1]{0,2,3,1:T(8,128)(2,1)S(1)} %bitcast.159, f32[2,1280,1024,2]{2,1,3,0:T(8,128)S(1)} %get-tuple-element.38, f32[2,2,1024]{2,1,0:T(2,128)S(1)} %exponential_add_fusion.2, f32[2,2,1024]{2,1,0:T(2,128)S(1)} %broadcast_maximum_fusion.2, pred[1024,1280]{0,1:T(8,128)(4,1)S(1)} %fusion.19), kind=kOutput, calls=%fused_computation.46 | convolution fusion | flops 697565184 | bytes 23166976 | tf_op jit(solution)/shard_map/kgqs,skd->qkgd/dot_general | solution.py:61
  179.6 42.1 %all-gather.13.cloned.1.call-done = bf16[3,2048,256]{2,1,0:T(8,128)(2,1)} async-done(((bf16[3,256,256]{2,1,0:T(8,128)(2,1)}), bf16[3,2048,256]{2,1,0:T(8,128)(2,1)}) %all-gather.13.cloned.1.call-update) | async-done | bytes 3145744 | tf_op jit(solution)/shard_map/all_gather | solution.py:87
  221.7 5.8 fusion.26
  227.5 70.2 %reduce-scatter.4.cloned.1.call-done = f32[256,2048]{1,0:T(8,128)} async-done(((f32[1024,2048]{1,0:T(8,128)}), f32[256,2048]{1,0:T(8,128)}) %reduce-scatter.4.cloned.1.call-update) | async-done | bytes 2097168 | tf_op jit(solution)/shard_map/reduce_scatter | solution.py:125
  297.7 2.7 convert_element_type.115
  300.4 0.2 reduce-scatter.6.cloned.1.call-start
  300.7 34.3 %all-gather.15.cloned.1.call-done = bf16[1024,2048]{1,0:T(8,128)(2,1)} async-done(((bf16[256,2048]{1,0:T(8,128)(2,1)}), bf16[1024,2048]{1,0:T(8,128)(2,1)}) %all-gather.15.cloned.1.call-update) | async-done | bytes 4194320 | tf_op jit(solution)/shard_map/all_gather | solution.py:128
  335.0 3.2 fusion.12
  338.3 0.2 copy-done.2
  338.5 1.0 fusion.14
  339.5 2.7 convolution_multiply_fusion.4
  342.3 1.5 convolution_convert_fusion.2
  343.9 3.4 collective-permute-start.3
  347.3 2.5 collective-permute-start.2
  349.8 2.5 convolution_multiply_fusion.1
  352.3 0.2 subtract_convert_fusion.1
  352.5 1.8 collective-permute-done.2
  354.4 0.8 fusion.52
  355.2 3.7 fusion.4
  358.9 4.7 fusion.1
  363.7 7.8 %fusion.23 = bf16[2,64,2,1024]{3,1,2,0:T(8,128)(2,1)} fusion(bf16[1280,2,64,1]{0,2,3,1:T(8,128)(2,1)} %bitcast.161, f32[2,1280,1024,2]{2,1,3,0:T(8,128)S(1)} %get-tuple-element.40, f32[2,2,1024]{2,1,0:T(2,128)S(1)} %exponential_add_fusion.1, f32[2,2,1024]{2,1,0:T(2,128)S(1)} %broadcast_maximum_fusion.1, pred[1024,1280]{0,1:T(8,128)(4,1)S(1)} %fusion.19), kind=kOutput, calls=%fused_computation.45 | convolution fusion | flops 697565184 | bytes 23166976 | tf_op jit(solution)/shard_map/kgqs,skd->qkgd/dot_general | solution.py:61
  371.5 5.9 %fusion.25 = f32[1024,2048]{1,0:T(8,128)} fusion(bf16[1024,256]{0,1:T(8,128)(2,1)} %bitcast.158, bf16[3,2048,256]{2,1,0:T(8,128)(2,1)} %all-gather.13.cloned.1.call-done), kind=kOutput, calls=%fused_computation.56 | convolution fusion | flops 1073741824 | bytes 9961472 | tf_op jit(solution)/shard_map/dot_general | solution.py:120
  377.5 70.6 %reduce-scatter.6.cloned.1.call-done = f32[256,2048]{1,0:T(8,128)} async-done(((f32[1024,2048]{1,0:T(8,128)}), f32[256,2048]{1,0:T(8,128)}) %reduce-scatter.6.cloned.1.call-update) | async-done | bytes 2097168 | tf_op jit(solution)/shard_map/reduce_scatter | solution.py:125
  448.1 2.7 convert_element_type.123
  450.8 0.3 reduce-scatter.8.cloned.1.call-start
  451.2 34.3 %all-gather.17.cloned.1.call-done = bf16[1024,2048]{1,0:T(8,128)(2,1)} async-done(((bf16[256,2048]{1,0:T(8,128)(2,1)}), bf16[1024,2048]{1,0:T(8,128)(2,1)}) %all-gather.17.cloned.1.call-update) | async-done | bytes 4194320 | tf_op jit(solution)/shard_map/all_gather | solution.py:128
  485.5 3.2 fusion.15
  488.7 0.2 copy-done.1
  488.9 1.0 fusion.17
  489.9 2.6 convolution_multiply_fusion.3
  492.6 1.5 convolution_convert_fusion.1
  494.2 3.4 collective-permute-start.5
  497.5 2.5 collective-permute-start.4
  500.0 2.5 convolution_multiply_fusion
  502.6 0.2 subtract_convert_fusion
  502.8 1.8 collective-permute-done.4
  504.7 3.7 fusion.5
  508.5 4.7 fusion.2
  513.3 6.2 %fusion.22 = bf16[2,64,2,1024]{3,1,2,0:T(8,128)(2,1)S(1)} fusion(bf16[1280,2,64,1]{0,2,3,1:T(8,128)(2,1)S(1)} %bitcast.160, f32[2,1280,1024,2]{2,1,3,0:T(8,128)S(1)} %get-tuple-element.42, f32[2,2,1024]{2,1,0:T(2,128)S(1)} %exponential_add_fusion, f32[2,2,1024]{2,1,0:T(2,128)S(1)} %broadcast_maximum_fusion, pred[1024,1280]{0,1:T(8,128)(4,1)S(1)} %fusion.19), kind=kOutput, calls=%fused_computation.44 | convolution fusion | flops 697565184 | bytes 23166976 | tf_op jit(solution)/shard_map/kgqs,skd->qkgd/dot_general | solution.py:61
  519.5 4.5 convolution_convert_fusion
  524.0 43.8 %reduce-scatter.8.cloned.1.call-done = bf16[256,2048]{1,0:T(8,128)(2,1)} async-done(((bf16[1024,2048]{1,0:T(8,128)(2,1)}), bf16[256,2048]{1,0:T(8,128)(2,1)}) %reduce-scatter.8.cloned.1.call-update) | async-done | bytes 1048592 | tf_op jit(solution)/shard_map/reduce_scatter | solution.py:130
  567.8 1.5 fusion.20
  569.4 2.8 fusion.21
  (57 shorter events, 1.8 us)
Async XLA Ops:
  6.5 48.4 %all-gather.7.cloned.1.call-start = ((), (), s32[]{:S(2)}) async-start(), calls=%async_computation.3 | async-start | bytes 1769472 | tf_op jit(solution)/shard_map/all_gather | solution.py:85
  7.3 92.4 %all-gather.9.cloned.1.call-start = ((), (), s32[]{:S(2)}) async-start(), calls=%async_computation.4 | async-start | bytes 1769472 | tf_op jit(solution)/shard_map/all_gather | solution.py:86
  8.0 152.9 %all-gather.11.cloned.1.call-start = ((), (), s32[]{:S(2)}) async-start(), calls=%async_computation.5 | async-start | bytes 3538944 | tf_op jit(solution)/shard_map/all_gather | solution.py:84
  8.7 212.9 %all-gather.13.cloned.1.call-start = ((), (), s32[]{:S(2)}) async-start(), calls=%async_computation.6 | async-start | bytes 3538944 | tf_op jit(solution)/shard_map/all_gather | solution.py:87
  9.3 288.4 %reduce-scatter.4.cloned.1.call-start = ((), (), s32[]{:S(2)}) async-start(), calls=%async_computation.7 | async-start | bytes 10485760 | tf_op jit(solution)/shard_map/reduce_scatter | solution.py:125
  9.4 4.4 copy-start
  19.5 90.3 %copy-start.5 = (f32[3,4]{1,0:T(4,128)S(1)}, f32[3,4]{1,0:T(4,128)}, u32[]{:S(2)}) copy-start(f32[3,4]{1,0:T(4,128)} %param.14) | copy-start | bytes 148
  103.5 6.4 %collective-permute-start.1 = (bf16[128,256]{0,1:T(8,128)(2,1)S(1)}, bf16[128,256]{0,1:T(8,128)(2,1)S(1)}, u32[]{:S(2)}, u32[]{:S(2)}) collective-permute-start(bf16[128,256]{0,1:T(8,128)(2,1)S(1)} %get-tuple-element.31), channel_id=1, source_target_pairs={{4,0},{8,4},{12,8},{16,12},{20,16},{24,20},{28,24},{5,1},{9,5},{13... | collective-permute-start | bytes 196616 | tf_op jit(solution)/shard_map/ppermute | solution.py:23
  106.0 8.4 %collective-permute-start = (bf16[128,256]{0,1:T(8,128)(2,1)S(1)}, bf16[128,256]{0,1:T(8,128)(2,1)S(1)}, u32[]{:S(2)}, u32[]{:S(2)}) collective-permute-start(bf16[128,256]{0,1:T(8,128)(2,1)S(1)} %get-tuple-element.30), channel_id=1, source_target_pairs={{0,4},{4,8},{8,12},{12,16},{16,20},{20,24},{24,28},{1,5},{5,9},{9,... | collective-permute-start | bytes 196616 | tf_op jit(solution)/shard_map/ppermute | solution.py:20
  227.5 107.6 %all-gather.15.cloned.1.call-start = ((), (), s32[]{:S(2)}) async-start(), calls=%async_computation.8 | async-start | bytes 5242880 | tf_op jit(solution)/shard_map/all_gather | solution.py:128
  300.4 147.7 %reduce-scatter.6.cloned.1.call-start = ((), (), s32[]{:S(2)}) async-start(), calls=%async_computation.9 | async-start | bytes 10485760 | tf_op jit(solution)/shard_map/reduce_scatter | solution.py:125
  335.0 3.4 copy-start.2
  339.5 2.8 copy-start.3
  343.9 8.6 %collective-permute-start.3 = (bf16[128,256]{0,1:T(8,128)(2,1)S(1)}, bf16[128,256]{0,1:T(8,128)(2,1)S(1)}, u32[]{:S(2)}, u32[]{:S(2)}) collective-permute-start(bf16[128,256]{0,1:T(8,128)(2,1)S(1)} %get-tuple-element.29), channel_id=1, source_target_pairs={{4,0},{8,4},{12,8},{16,12},{20,16},{24,20},{28,24},{5,1},{9,5},{13... | collective-permute-start | bytes 196616 | tf_op jit(solution)/shard_map/ppermute | solution.py:23
  347.3 7.1 %collective-permute-start.2 = (bf16[128,256]{0,1:T(8,128)(2,1)S(1)}, bf16[128,256]{0,1:T(8,128)(2,1)S(1)}, u32[]{:S(2)}, u32[]{:S(2)}) collective-permute-start(bf16[128,256]{0,1:T(8,128)(2,1)S(1)} %get-tuple-element.28), channel_id=1, source_target_pairs={{0,4},{4,8},{8,12},{12,16},{16,20},{20,24},{24,28},{1,5},{5,9},{9,... | collective-permute-start | bytes 196616 | tf_op jit(solution)/shard_map/ppermute | solution.py:20
  377.5 108.0 %all-gather.17.cloned.1.call-start = ((), (), s32[]{:S(2)}) async-start(), calls=%async_computation.10 | async-start | bytes 5242880 | tf_op jit(solution)/shard_map/all_gather | solution.py:128
  450.8 117.0 %reduce-scatter.8.cloned.1.call-start = ((), (), s32[]{:S(2)}) async-start(), calls=%async_computation.11 | async-start | bytes 5242880 | tf_op jit(solution)/shard_map/reduce_scatter | solution.py:130
  485.5 3.4 copy-start.1
  494.2 8.6 %collective-permute-start.5 = (bf16[128,256]{0,1:T(8,128)(2,1)S(1)}, bf16[128,256]{0,1:T(8,128)(2,1)S(1)}, u32[]{:S(2)}, u32[]{:S(2)}) collective-permute-start(bf16[128,256]{0,1:T(8,128)(2,1)S(1)} %get-tuple-element.27), channel_id=1, source_target_pairs={{4,0},{8,4},{12,8},{16,12},{20,16},{24,20},{28,24},{5,1},{9,5},{13... | collective-permute-start | bytes 196616 | tf_op jit(solution)/shard_map/ppermute | solution.py:23
  497.5 7.1 %collective-permute-start.4 = (bf16[128,256]{0,1:T(8,128)(2,1)S(1)}, bf16[128,256]{0,1:T(8,128)(2,1)S(1)}, u32[]{:S(2)}, u32[]{:S(2)}) collective-permute-start(bf16[128,256]{0,1:T(8,128)(2,1)S(1)} %get-tuple-element.26), channel_id=1, source_target_pairs={{0,4},{4,8},{8,12},{12,16},{16,20},{20,24},{24,28},{1,5},{5,9},{9,... | collective-permute-start | bytes 196616 | tf_op jit(solution)/shard_map/ppermute | solution.py:20
  519.5 49.9 %copy-start.4 = (f32[2048]{0:T(1024)S(1)}, f32[2048]{0:T(1024)}, u32[]{:S(2)}) copy-start(f32[2048]{0:T(1024)} %param.15) | copy-start | bytes 24580
Sparse Core Ops, SparseCore 0:
  9.5 45.3 all-gather.6
  57.1 42.5 all-gather.8
  101.8 58.9 all-gather.10
  162.9 58.7 all-gather.12
  227.6 70.0 reduce-scatter.3
  300.5 34.4 all-gather.14
  377.6 70.4 reduce-scatter.5
  450.9 34.4 all-gather.16
  524.1 43.6 reduce-scatter.7
where the time goes:
time: 586 us; the launch traced here: 579 us
  waiting for transfers between devices  429 us (73%)
  matrix products  72.3 us (12%)
  other arithmetic  42.9 us (7%)
  starting transfers between devices  18.7 us (3%)
  between operations  13.9 us (2%)
    reduce_scatter x2, waiting for transfers between devices, shards(): lax.psum_scatter(project(), 'tp', scatter_dimension=0, tiled=True)  141 us
    all_gather x2, waiting for transfers between devices, shards(): current = lax.all_gather(share_rows, 'tp', axis=0, tiled=True)  68.6 us
    all_gather x1, waiting for transfers between devices, shards(): lax.all_gather(query_weight, 'sp', axis=1, tiled=True)  46.3 us
    reduce_scatter x1, waiting for transfers between devices, shards(): lax.psum_scatter(project().astype(jnp.bfloat16), 'tp', scatter_dimension=...  43.8 us
    all_gather x1, waiting for transfers between devices, shards(): lax.all_gather(output_weight, 'sp', axis=1, tiled=True)  42.1 us
    all_gather x1, waiting for transfers between devices, shards(): lax.all_gather(value_weight, 'sp', axis=1, tiled=True)  40.8 us
    all_gather x1, waiting for transfers between devices, shards(): lax.all_gather(key_weight, 'sp', axis=1, tiled=True)  35.3 us
    dot_general x3, matrix products, attend(): jnp.einsum('kgqs,skd->qkgd', weights, value_rows, preferred_element_type=...  20.2 us
  transfers between devices with their start and end apart: 15, of which 12 were waited for; matrix products, arithmetic and copies ran while one was open for 7% of the time, Pallas kernels for 0%

commit v1 on v0

v1 whole, which is shorter than its diff:
```python
import functools

import jax
import jax.numpy as jnp
from jax import lax
from jax.experimental import pallas as pl
from jax.experimental.pallas import tpu as pltpu
from jax.sharding import PartitionSpec as P

HEAD_DIM = 64
WINDOW = 128
EPS = 1e-06
AXES = ("sp", "tp")
F32 = jnp.float32
BF16 = jnp.bfloat16
VMEM_LIMIT = 48 * 1024 * 1024


def project_kernel(cur_ref, gain_ref, w_ref, cos_ref, sin_ref, q_ref, kv_ref, normed):
    @pl.when(pl.program_id(0) == 0)
    def _():
        wide = cur_ref[...].astype(F32)
        inv_root = lax.rsqrt(jnp.mean(wide * wide, axis=-1, keepdims=True) + EPS)
        normed[...] = (wide * inv_root * gain_ref[...]).astype(BF16)

    pieces, rows, width = w_ref.shape[0], w_ref.shape[3], w_ref.shape[4]
    acc = jnp.zeros((cur_ref.shape[0], width), F32)
    for s in range(pieces):
        acc += jnp.dot(
            normed[:, s * rows : (s + 1) * rows], w_ref[s, 0, 0], preferred_element_type=F32
        )
    half = HEAD_DIM // 2
    lane = lax.broadcasted_iota(jnp.int32, acc.shape, 1)
    front = (lane % HEAD_DIM) < half
    partner = jnp.where(front, pltpu.roll(acc, width - half, 1), pltpu.roll(acc, half, 1))
    turned = (acc * cos_ref[...] + partner * sin_ref[...]).astype(BF16)
    q_ref[0] = turned[:, : width // 2]
    kv_ref[0] = turned[:, width // 2 :]


def attend_kernel(layer, last, seq_total, sink_ref, off_ref, q_ref, kv_ref, lo_ref, hi_ref, w_ref, gain_ref, out_ref, acc):
    t = pl.program_id(0)
    tokens, cols = q_ref.shape[1], q_ref.shape[2]
    heads = cols // HEAD_DIM
    kv_cols = kv_ref.shape[2] // 2
    groups = kv_cols // HEAD_DIM
    per_group = heads // groups
    block = WINDOW
    span = block + 2 * WINDOW
    keys = jnp.concatenate([lo_ref[0], kv_ref[0], hi_ref[0]], axis=0)
    q_all = q_ref[0]
    i_pos = lax.broadcasted_iota(jnp.int32, (per_group * block, span), 0) % block
    j_pos = lax.broadcasted_iota(jnp.int32, (per_group * block, span), 1) - WINDOW
    near = jnp.abs(i_pos - j_pos) <= WINDOW
    row_head = lax.broadcasted_iota(jnp.int32, (per_group * block, 1), 0) // block
    parts = []
    for b in range(tokens // block):
        key_pos = off_ref[0] + b * block + j_pos
        allowed = near & (key_pos >= 0) & (key_pos < seq_total)
        heads_out = []
        for g in range(groups):
            lanes = slice(g * HEAD_DIM, (g + 1) * HEAD_DIM)
            here = slice(b * block, b * block + span)
            k = keys[here, lanes]
            v = keys[here, kv_cols + g * HEAD_DIM : kv_cols + (g + 1) * HEAD_DIM]
            q = jnp.concatenate(
                [
                    q_all[b * block : (b + 1) * block, h * HEAD_DIM : (h + 1) * HEAD_DIM]
                    for h in range(g * per_group, (g + 1) * per_group)
                ],
                axis=0,
            )
            scores = lax.dot_general(q, k, (((1,), (1,)), ((), ())), preferred_element_type=F32)
            scores = jnp.where(allowed, scores, -jnp.inf)
            sink = jnp.zeros((per_group * block, 1), F32)
            for e in range(per_group):
                sink = jnp.where(row_head == e, sink_ref[layer, t * heads + g * per_group + e], sink)
            largest = jnp.maximum(jnp.max(scores, axis=-1, keepdims=True), sink)
            powers = jnp.exp(scores - largest)
            total = jnp.sum(powers, axis=-1, keepdims=True) + jnp.exp(sink - largest)
            weights = (powers * (1.0 / total)).astype(BF16)
            mixed = jnp.dot(weights, v, preferred_element_type=F32).astype(BF16)
            heads_out += [mixed[e * block : (e + 1) * block] for e in range(per_group)]
        parts.append(jnp.concatenate(heads_out, axis=1))
    attended = jnp.concatenate(parts, axis=0)
    rows = w_ref.shape[3]
    for s in range(w_ref.shape[0]):
        piece = lax.dot_general(
            attended, w_ref[s, 0, 0], (((1,), (1,)), ((), ())), preferred_element_type=F32
        )
        where = slice(s * rows, (s + 1) * rows)

        @pl.when(t == 0)
        def _():
            acc[:, where] = piece

        @pl.when(t > 0)
        def _():
            acc[:, where] += piece

    @pl.when(t == pl.num_programs(0) - 1)
    def _():
        state = acc[...].astype(BF16)
        if last:
            wide = state.astype(F32)
            inv_root = lax.rsqrt(jnp.mean(wide * wide, axis=-1, keepdims=True) + EPS)
            out_ref[...] = wide * inv_root * gain_ref[...]
        else:
            out_ref[...] = state


def gather_weights(packed):
    count = lax.axis_size("sp") * lax.axis_size("tp")
    whole = lax.all_gather(packed, AXES, axis=0, tiled=False)
    return whole.reshape((lax.axis_size("sp"), lax.axis_size("tp")) + packed.shape)


def shards(
    inputs, norm_gain, query_weight, key_weight, value_weight, output_weight, sink_logit, final_gain
):
    n_sp, n_tp = lax.axis_size("sp"), lax.axis_size("tp")
    layers, rows, cols = query_weight.shape
    features = inputs.shape[1]
    tokens = inputs.shape[0] // n_tp
    width = 2 * cols
    place = lax.axis_index("sp") * n_tp + lax.axis_index("tp")
    offset = place * tokens
    seq_total = tokens * n_sp * n_tp
    whole = gather_weights(
        jnp.concatenate([query_weight, key_weight, value_weight, output_weight], axis=2)
    )
    sinks = lax.all_gather(sink_logit, "tp", axis=1, tiled=True)

    half = HEAD_DIM // 2
    inverse = 10000.0 ** (-jnp.arange(half).astype(F32) / half)
    places = (offset + jnp.arange(tokens, dtype=jnp.int32)).astype(F32)
    angles = places[:, None] * inverse[None, :]
    cosine, sine = jnp.cos(angles), jnp.sin(angles)
    scale = float(features) ** (-0.5)
    root = HEAD_DIM ** (-0.5)
    pair_c = jnp.concatenate([cosine, cosine], axis=1) * scale
    pair_s = jnp.concatenate([-sine, sine], axis=1) * scale
    kv_cols = key_weight.shape[2]
    heads, groups = cols // HEAD_DIM, kv_cols // HEAD_DIM
    one = jnp.ones((tokens, kv_cols), F32)
    cos_table = jnp.concatenate([jnp.tile(pair_c * root, (1, heads)), jnp.tile(pair_c, (1, groups)), one], axis=1)
    sin_table = jnp.concatenate([jnp.tile(pair_s * root, (1, heads)), jnp.tile(pair_s, (1, groups)), 0 * one], axis=1)
    offset_row = jnp.reshape(offset, (1,)).astype(jnp.int32)

    count = n_sp * n_tp
    forward = [(i, i + 1) for i in range(count - 1)]
    backward = [(b, a) for a, b in forward]
    current = lax.dynamic_slice_in_dim(inputs, lax.axis_index("tp") * tokens, tokens, 0)
    full = lambda *shape: pl.BlockSpec(shape, lambda t: (0,) * len(shape))
    smem = pl.BlockSpec(memory_space=pltpu.SMEM)
    for layer in range(layers):
        last = layer == layers - 1
        queries, kv = pl.pallas_call(
            project_kernel,
            name="project",
            grid=(n_tp,),
            out_shape=[jax.ShapeDtypeStruct((n_tp, tokens, cols), BF16)] * 2,
            in_specs=[
                full(tokens, features),
                full(1, features),
                pl.BlockSpec((n_sp, 1, 1, rows, width), lambda t, l=layer: (0, t, l, 0, 0)),
                full(tokens, width),
                full(tokens, width),
            ],
            out_specs=[pl.BlockSpec((1, tokens, cols), lambda t: (t, 0, 0))] * 2,
            scratch_shapes=[pltpu.VMEM((tokens, features), BF16)],
            compiler_params=pltpu.CompilerParams(vmem_limit_bytes=VMEM_LIMIT),
        )(current, norm_gain[layer : layer + 1], whole, cos_table, sin_table)
        low = lax.ppermute(kv[:, tokens - WINDOW :], AXES, forward)
        high = lax.ppermute(kv[:, :WINDOW], AXES, backward)
        current = pl.pallas_call(
            functools.partial(attend_kernel, layer, last, seq_total),
            name="attend",
            grid=(n_tp,),
            out_shape=jax.ShapeDtypeStruct((tokens, features), F32 if last else BF16),
            in_specs=[
                smem,
                smem,
                pl.BlockSpec((1, tokens, cols), lambda t: (t, 0, 0)),
                pl.BlockSpec((1, tokens, cols), lambda t: (t, 0, 0)),
                pl.BlockSpec((1, WINDOW, cols), lambda t: (t, 0, 0)),
                pl.BlockSpec((1, WINDOW, cols), lambda t: (t, 0, 0)),
                pl.BlockSpec((n_sp, 1, 1, rows, cols), lambda t, l=layer: (0, t, l, 0, 2)),
                full(1, features),
            ],
            out_specs=full(tokens, features),
            scratch_shapes=[pltpu.VMEM((tokens, features), F32)],
            compiler_params=pltpu.CompilerParams(vmem_limit_bytes=VMEM_LIMIT),
        )(sinks, offset_row, queries, kv, low, high, whole, final_gain[None])
    return current


def solution(mesh):
    in_specs = (
        P("sp", None),
        P(),
        P(None, "sp", "tp"),
        P(None, "sp", "tp"),
        P(None, "sp", "tp"),
        P(None, "sp", "tp"),
        P(None, "tp"),
        P(),
    )
    out_specs = P(("sp", "tp"), None)
    return jax.shard_map(shards, mesh=mesh, in_specs=in_specs, out_specs=out_specs, check_vma=False)
```

time: 586 us -> 345 us (0.59); the launches traced: 579 us -> 344 us
  waiting for transfers between devices: 429 us -> 229 us
  Pallas kernels: 0 us -> 74.9 us
  matrix products: 72.3 us -> 0 us
  other arithmetic: 42.9 us -> 2.74 us
    reduce_scatter x3 -> x0, waiting for transfers between devices: 185 us -> none  [the longest x2 141 us: shards(): lax.psum_scatter(project(), 'tp', scatter_dimension=0, tiled=True)]
    pallas_call x0 -> x6, Pallas kernels: none -> 74.9 us  [the longest x3 54.4 us: shards(): pl.pallas_call(functools.partial(attend_kernel, layer, last, seq_total),...]
    dot_general x18 -> x0, matrix products: 72.3 us -> none  [the longest x3 20.2 us: attend(): jnp.einsum('kgqs,skd->qkgd', weights, value_rows, preferred_element_type=...]
    reduce_sum x7 -> x0, other arithmetic: 25.3 us -> none  [the longest x3 14 us: attend(): denominator = jnp.sum(powers, axis=-1) + jnp.exp(sink_col - largest)]
    all_gather x6 -> x1, waiting for transfers between devices: 233 us -> 213 us  [gather_weights(): whole = lax.all_gather(packed, AXES, axis=0, tiled=False)]
    convert_element_type x5 -> x1, other arithmetic: 10.5 us -> 0.01 us  [shards(): places = (offset + jnp.arange(tokens, dtype=jnp.int32)).astype(F32)]
    ppermute x6, waiting for transfers between devices: 8.13 us -> 16.3 us  [the longest x3 13 us: shards(): low = lax.ppermute(kv[:, tokens - WINDOW:], AXES, forward)]
  transfers between devices with their start and end apart: 15 -> 7, of which waited for: 12 -> 6; matrix products, arithmetic and copies ran while one was open for 7% -> 1% of each run, Pallas kernels for 0% -> 0%
where the time goes in v1:
time: 345 us; the launch traced here: 344 us
  waiting for transfers between devices  229 us (66%)
  Pallas kernels  74.9 us (22%)
  starting transfers between devices  16.6 us (5%)
  between operations  13.7 us (4%)
  blocking collectives  5.52 us (2%)
    all_gather x1, waiting for transfers between devices, gather_weights(): whole = lax.all_gather(packed, AXES, axis=0, tiled=False)  213 us
    pallas_call x3, Pallas kernels, shards(): pl.pallas_call(functools.partial(attend_kernel, layer, last, seq_total),...  54.4 us
    pallas_call x3, Pallas kernels, shards(): pl.pallas_call(project_kernel, name='project', grid=(n_tp,), out_shape=[j...  20.5 us
    ppermute x3, waiting for transfers between devices, shards(): low = lax.ppermute(kv[:, tokens - WINDOW:], AXES, forward)  13 us
    ppermute x3, starting transfers between devices, shards(): high = lax.ppermute(kv[:, :WINDOW], AXES, backward)  10.1 us
  transfers between devices with their start and end apart: 7, of which 6 were waited for; matrix products, arithmetic and copies ran while one was open for 1% of the time, Pallas kernels for 0%

profile of v1, /device:TPU:8, one launch (start us, length us, event | category | flops | bytes accessed | tf_op | source)
XLA Modules:
  0.0 344.4 jit_solution(16320520198270471167)
XLA Ops:
  6.5 0.0 all-gather.4.cloned.1.call-start
  6.5 2.4 pad_maximum_fusion
  8.9 0.0 all-gather.4.cloned.1.call-update
  9.0 0.2 fusion.4
  9.3 0.1 copy.20
  9.4 0.1 copy.22
  9.5 0.1 copy.19
  9.7 0.0 copy-start.1
  9.7 0.1 copy.21
  9.8 0.1 maximum_maximum_fusion.cos_ref
  9.9 0.1 maximum_maximum_fusion.1.sin_ref
  10.0 1.3 constant_dynamic-slice_fusion.cur_ref
  11.3 0.0 copy-done.1
  11.3 212.6 %all-gather.4.cloned.1.call-done = bf16[96,256,768]{2,1,0:T(8,128)(2,1)} async-done(((bf16[3,256,768]{2,1,0:T(8,128)(2,1)}), bf16[96,256,768]{2,1,0:T(8,128)(2,1)}) %all-gather.4.cloned.1.call-update) | async-done | bytes 37748752 | tf_op jit(solution)/shard_map/all_gather | solution.py:114
  223.9 0.0 copy-start.2
  223.9 0.0 copy-start
  223.9 6.8 %project.3 = (bf16[4,256,256]{2,1,0:T(8,128)(2,1)S(1)}, bf16[4,256,256]{2,1,0:T(8,128)(2,1)S(1)}) custom-call(bf16[256,2048]{1,0:T(8,128)(2,1)S(1)} %constant_dynamic-slice_fusion.cur_ref, f32[1,2048]{1,0:T(1,128)S(1)} %get-tuple-element.26.gain_ref, bf16[8,4,3,256,768]{4,3,2,1,0:T(8,128)(2,1)} %bitcast.17, f32[256,512]{1,0:T(8,128)S(1)} %maximum_maximum_fusion.cos_ref, ...), custom_call_target="tpu_custom_call" | custom-call | tf_op jit(solution)/shard_map/project/pallas_call | solution.py:158
  230.8 5.1 %collective-permute-start.1 = (bf16[4,128,256]{2,1,0:T(8,128)(2,1)S(1)}, bf16[4,128,256]{2,1,0:T(8,128)(2,1)S(1)}, u32[]{:S(2)}, u32[]{:S(2)}) collective-permute-start(bf16[4,128,256]{2,1,0:T(8,128)(2,1)S(1)} %get-tuple-element.21), channel_id=1, source_target_pairs={{1,0},{2,1},{3,2},{4,3},{5,4},{6,5},{7,6},{8,7},{9,8},{10,9},{11,1... | collective-permute-start | bytes 786440 | tf_op jit(solution)/shard_map/ppermute | solution.py:175
  235.9 1.9 collective-permute-start
  237.8 0.0 copy-done.2
  237.8 0.1 copy.17
  237.9 5.5 %all-gather.1 = f32[4,4,3]{2,1,0:T(4,128)S(1)} all-gather(f32[1,4,3]{2,1,0:T(4,128)S(1)} %bitcast.28), channel_id=1, replica_groups=mesh['sp'=8,'tp'=4] {'tp'}, dimensions={0}, use_global_device_ids=true | all-gather | bytes 240 | tf_op jit(solution)/shard_map/all_gather | solution.py:132
  243.4 0.1 copy.23
  243.5 0.0 collective-permute-done.1.hi_ref
  243.5 1.9 collective-permute-done.lo_ref
  245.4 0.0 copy-done
  245.4 17.6 %attend.3.cur_ref = bf16[256,2048]{1,0:T(8,128)(2,1)S(1)} custom-call(f32[3,16]{1,0:T(4,128)S(1)} %bitcast.14, s32[1]{0:T(128)} %bitcast.4.off_ref, bf16[4,256,256]{2,1,0:T(8,128)(2,1)S(1)} %get-tuple-element.11.q_ref, bf16[4,256,256]{2,1,0:T(8,128)(2,1)S(1)} %get-tuple-element.12.kv_ref, bf16[4,128,256]{2,1,0:T(8,128)(2,1)S(1)} %collective-permute-done.lo_ref, ...), custom_call_target="tpu_custom_call" | custom-call | tf_op jit(solution)/shard_map/attend/pallas_call | solution.py:176
  263.0 6.8 %project.4 = (bf16[4,256,256]{2,1,0:T(8,128)(2,1)S(1)}, bf16[4,256,256]{2,1,0:T(8,128)(2,1)S(1)}) custom-call(bf16[256,2048]{1,0:T(8,128)(2,1)S(1)} %attend.3.cur_ref, f32[1,2048]{1,0:T(1,128)S(1)} %get-tuple-element.27.gain_ref, bf16[8,4,3,256,768]{4,3,2,1,0:T(8,128)(2,1)} %bitcast.19, f32[256,512]{1,0:T(8,128)S(1)} %maximum_maximum_fusion.cos_ref, ...), custom_call_target="tpu_custom_call" | custom-call | tf_op jit(solution)/shard_map/project/pallas_call | solution.py:158
  269.8 3.1 collective-permute-start.3
  273.0 1.9 collective-permute-start.2
  274.9 2.0 collective-permute-done.3.hi_ref
  276.9 5.6 %collective-permute-done.2.lo_ref = bf16[4,128,256]{2,1,0:T(8,128)(2,1)S(1)} collective-permute-done((bf16[4,128,256]{2,1,0:T(8,128)(2,1)S(1)}, bf16[4,128,256]{2,1,0:T(8,128)(2,1)S(1)}, u32[]{:S(2)}, u32[]{:S(2)}) %collective-permute-start.2) | collective-permute-done | bytes 262176 | tf_op jit(solution)/shard_map/ppermute | solution.py:174
  282.5 17.6 %attend.4.cur_ref = bf16[256,2048]{1,0:T(8,128)(2,1)S(1)} custom-call(f32[3,16]{1,0:T(4,128)S(1)} %bitcast.15, s32[1]{0:T(128)} %bitcast.4.off_ref, bf16[4,256,256]{2,1,0:T(8,128)(2,1)S(1)} %get-tuple-element.13.q_ref, bf16[4,256,256]{2,1,0:T(8,128)(2,1)S(1)} %get-tuple-element.14.kv_ref, bf16[4,128,256]{2,1,0:T(8,128)(2,1)S(1)} %collective-permute-done.2.lo_ref, ...), custom_call_target="tpu_custom_call" | custom-call | tf_op jit(solution)/shard_map/attend/pallas_call | solution.py:176
  300.1 6.8 %project.5 = (bf16[4,256,256]{2,1,0:T(8,128)(2,1)S(1)}, bf16[4,256,256]{2,1,0:T(8,128)(2,1)S(1)}) custom-call(bf16[256,2048]{1,0:T(8,128)(2,1)S(1)} %attend.4.cur_ref, f32[1,2048]{1,0:T(1,128)S(1)} %get-tuple-element.25.gain_ref, bf16[8,4,3,256,768]{4,3,2,1,0:T(8,128)(2,1)} %bitcast.21, f32[256,512]{1,0:T(8,128)S(1)} %maximum_maximum_fusion.cos_ref, ...), custom_call_target="tpu_custom_call" | custom-call | tf_op jit(solution)/shard_map/project/pallas_call | solution.py:158
  307.0 1.9 collective-permute-start.5
  308.9 2.6 collective-permute-start.4
  311.5 1.3 collective-permute-done.5.hi_ref
  312.8 5.6 %collective-permute-done.4.lo_ref = bf16[4,128,256]{2,1,0:T(8,128)(2,1)S(1)} collective-permute-done((bf16[4,128,256]{2,1,0:T(8,128)(2,1)S(1)}, bf16[4,128,256]{2,1,0:T(8,128)(2,1)S(1)}, u32[]{:S(2)}, u32[]{:S(2)}) %collective-permute-start.4) | collective-permute-done | bytes 262176 | tf_op jit(solution)/shard_map/ppermute | solution.py:174
  318.4 19.2 %attend.5 = f32[256,2048]{1,0:T(8,128)} custom-call(f32[3,16]{1,0:T(4,128)S(1)} %bitcast.16, s32[1]{0:T(128)} %bitcast.4.off_ref, bf16[4,256,256]{2,1,0:T(8,128)(2,1)S(1)} %get-tuple-element.15.q_ref, bf16[4,256,256]{2,1,0:T(8,128)(2,1)S(1)} %get-tuple-element.16.kv_ref, bf16[4,128,256]{2,1,0:T(8,128)(2,1)S(1)} %collective-permute-done.4.lo_ref, ...), custom_call_target="tpu_custom_call" | custom-call | tf_op jit(solution)/shard_map/attend/pallas_call | solution.py:176
  (15 shorter events, 0.2 us)
Async XLA Ops:
  6.5 217.4 %all-gather.4.cloned.1.call-start = ((), (), s32[]{:S(2)}) async-start(), calls=%async_computation | async-start | bytes 38928384 | tf_op jit(solution)/shard_map/all_gather | solution.py:114
  9.7 1.6 copy-start.1
  223.9 13.9 %copy-start.2 = (f32[3,4]{1,0:T(4,128)S(1)}, f32[3,4]{1,0:T(4,128)}, u32[]{:S(2)}) copy-start(f32[3,4]{1,0:T(4,128)} %param.14) | copy-start | bytes 148
  223.9 21.4 %copy-start = (f32[2048]{0:T(1024)S(1)}, f32[2048]{0:T(1024)}, u32[]{:S(2)}) copy-start(f32[2048]{0:T(1024)} %param.15) | copy-start | bytes 24580
  230.8 12.7 %collective-permute-start.1 = (bf16[4,128,256]{2,1,0:T(8,128)(2,1)S(1)}, bf16[4,128,256]{2,1,0:T(8,128)(2,1)S(1)}, u32[]{:S(2)}, u32[]{:S(2)}) collective-permute-start(bf16[4,128,256]{2,1,0:T(8,128)(2,1)S(1)} %get-tuple-element.21), channel_id=1, source_target_pairs={{1,0},{2,1},{3,2},{4,3},{5,4},{6,5},{7,6},{8,7},{9,8},{10,9},{11,1... | collective-permute-start | bytes 786440 | tf_op jit(solution)/shard_map/ppermute | solution.py:175
  235.9 9.5 %collective-permute-start = (bf16[4,128,256]{2,1,0:T(8,128)(2,1)S(1)}, bf16[4,128,256]{2,1,0:T(8,128)(2,1)S(1)}, u32[]{:S(2)}, u32[]{:S(2)}) collective-permute-start(bf16[4,128,256]{2,1,0:T(8,128)(2,1)S(1)} %get-tuple-element.22), channel_id=1, source_target_pairs={{0,1},{1,2},{2,3},{3,4},{4,5},{5,6},{6,7},{7,8},{8,9},{9,10},{10,1... | collective-permute-start | bytes 786440 | tf_op jit(solution)/shard_map/ppermute | solution.py:174
  269.8 7.1 %collective-permute-start.3 = (bf16[4,128,256]{2,1,0:T(8,128)(2,1)S(1)}, bf16[4,128,256]{2,1,0:T(8,128)(2,1)S(1)}, u32[]{:S(2)}, u32[]{:S(2)}) collective-permute-start(bf16[4,128,256]{2,1,0:T(8,128)(2,1)S(1)} %get-tuple-element.19), channel_id=1, source_target_pairs={{1,0},{2,1},{3,2},{4,3},{5,4},{6,5},{7,6},{8,7},{9,8},{10,9},{11,1... | collective-permute-start | bytes 786440 | tf_op jit(solution)/shard_map/ppermute | solution.py:175
  273.0 9.5 %collective-permute-start.2 = (bf16[4,128,256]{2,1,0:T(8,128)(2,1)S(1)}, bf16[4,128,256]{2,1,0:T(8,128)(2,1)S(1)}, u32[]{:S(2)}, u32[]{:S(2)}) collective-permute-start(bf16[4,128,256]{2,1,0:T(8,128)(2,1)S(1)} %get-tuple-element.20), channel_id=1, source_target_pairs={{0,1},{1,2},{2,3},{3,4},{4,5},{5,6},{6,7},{7,8},{8,9},{9,10},{10,1... | collective-permute-start | bytes 786440 | tf_op jit(solution)/shard_map/ppermute | solution.py:174
  307.0 5.8 %collective-permute-start.5 = (bf16[4,128,256]{2,1,0:T(8,128)(2,1)S(1)}, bf16[4,128,256]{2,1,0:T(8,128)(2,1)S(1)}, u32[]{:S(2)}, u32[]{:S(2)}) collective-permute-start(bf16[4,128,256]{2,1,0:T(8,128)(2,1)S(1)} %get-tuple-element.17), channel_id=1, source_target_pairs={{1,0},{2,1},{3,2},{4,3},{5,4},{6,5},{7,6},{8,7},{9,8},{10,9},{11,1... | collective-permute-start | bytes 786440 | tf_op jit(solution)/shard_map/ppermute | solution.py:175
  308.9 9.5 %collective-permute-start.4 = (bf16[4,128,256]{2,1,0:T(8,128)(2,1)S(1)}, bf16[4,128,256]{2,1,0:T(8,128)(2,1)S(1)}, u32[]{:S(2)}, u32[]{:S(2)}) collective-permute-start(bf16[4,128,256]{2,1,0:T(8,128)(2,1)S(1)} %get-tuple-element.18), channel_id=1, source_target_pairs={{0,1},{1,2},{2,3},{3,4},{4,5},{5,6},{6,7},{7,8},{8,9},{9,10},{10,1... | collective-permute-start | bytes 786440 | tf_op jit(solution)/shard_map/ppermute | solution.py:174
Sparse Core Ops, SparseCore 0:
  10.2 213.6 all-gather.3

commit v2 on v1

--- a/solution.py
+++ b/solution.py
@@ -38,9 +38,17 @@
     kv_ref[0] = turned[:, width // 2 :]
 
 
-def attend_kernel(layer, last, seq_total, sink_ref, off_ref, q_ref, kv_ref, lo_ref, hi_ref, w_ref, gain_ref, out_ref, acc):
+def attend_kernel(layer, last, sink_ref, q_ref, kv_ref, lo_ref, hi_ref, bias_ref, whole_ref, gain_ref, out_ref, w_ref, attended, acc, w_sem):
     t = pl.program_id(0)
     tokens, cols = q_ref.shape[1], q_ref.shape[2]
+    load = pltpu.make_async_copy(
+        whole_ref.at[:, :, layer, :, pl.ds(2 * cols, cols)], w_ref, w_sem
+    )
+
+    @pl.when(t == 0)
+    def _():
+        load.start()
+
     heads = cols // HEAD_DIM
     kv_cols = kv_ref.shape[2] // 2
     groups = kv_cols // HEAD_DIM
@@ -49,64 +57,55 @@
     span = block + 2 * WINDOW
     keys = jnp.concatenate([lo_ref[0], kv_ref[0], hi_ref[0]], axis=0)
     q_all = q_ref[0]
-    i_pos = lax.broadcasted_iota(jnp.int32, (per_group * block, span), 0) % block
-    j_pos = lax.broadcasted_iota(jnp.int32, (per_group * block, span), 1) - WINDOW
-    near = jnp.abs(i_pos - j_pos) <= WINDOW
     row_head = lax.broadcasted_iota(jnp.int32, (per_group * block, 1), 0) // block
-    parts = []
     for b in range(tokens // block):
-        key_pos = off_ref[0] + b * block + j_pos
-        allowed = near & (key_pos >= 0) & (key_pos < seq_total)
-        heads_out = []
+        here = slice(b * block, (b + 1) * block)
+        bias = jnp.concatenate([bias_ref[here]] * per_group, axis=0)
+        near = slice(b * block, b * block + span)
         for g in range(groups):
-            lanes = slice(g * HEAD_DIM, (g + 1) * HEAD_DIM)
-            here = slice(b * block, b * block + span)
-            k = keys[here, lanes]
-            v = keys[here, kv_cols + g * HEAD_DIM : kv_cols + (g + 1) * HEAD_DIM]
+            k = keys[near, g * HEAD_DIM : (g + 1) * HEAD_DIM]
+            v = keys[near, kv_cols + g * HEAD_DIM : kv_cols + (g + 1) * HEAD_DIM]
+            first = g * per_group
             q = jnp.concatenate(
                 [
-                    q_all[b * block : (b + 1) * block, h * HEAD_DIM : (h + 1) * HEAD_DIM]
-                    for h in range(g * per_group, (g + 1) * per_group)
+                    q_all[here, h * HEAD_DIM : (h + 1) * HEAD_DIM]
+                    for h in range(first, first + per_group)
                 ],
                 axis=0,
             )
             scores = lax.dot_general(q, k, (((1,), (1,)), ((), ())), preferred_element_type=F32)
-            scores = jnp.where(allowed, scores, -jnp.inf)
+            scores = scores + bias
             sink = jnp.zeros((per_group * block, 1), F32)
             for e in range(per_group):
-                sink = jnp.where(row_head == e, sink_ref[layer, t * heads + g * per_group + e], sink)
+                sink = jnp.where(row_head == e, sink_ref[layer, t * heads + first + e], sink)
             largest = jnp.maximum(jnp.max(scores, axis=-1, keepdims=True), sink)
             powers = jnp.exp(scores - largest)
             total = jnp.sum(powers, axis=-1, keepdims=True) + jnp.exp(sink - largest)
-            weights = (powers * (1.0 / total)).astype(BF16)
-            mixed = jnp.dot(weights, v, preferred_element_type=F32).astype(BF16)
-            heads_out += [mixed[e * block : (e + 1) * block] for e in range(per_group)]
-        parts.append(jnp.concatenate(heads_out, axis=1))
-    attended = jnp.concatenate(parts, axis=0)
-    rows = w_ref.shape[3]
-    for s in range(w_ref.shape[0]):
-        piece = lax.dot_general(
-            attended, w_ref[s, 0, 0], (((1,), (1,)), ((), ())), preferred_element_type=F32
-        )
-        where = slice(s * rows, (s + 1) * rows)
-
-        @pl.when(t == 0)
-        def _():
-            acc[:, where] = piece
-
-        @pl.when(t > 0)
-        def _():
-            acc[:, where] += piece
+            mixed = jnp.dot(powers.astype(BF16), v, preferred_element_type=F32) * (1.0 / total)
+            mixed = mixed.astype(BF16)
+            attended[t, here, first * HEAD_DIM : (first + per_group) * HEAD_DIM] = jnp.concatenate(
+                [mixed[e * block : (e + 1) * block] for e in range(per_group)], axis=1
+            )
 
     @pl.when(t == pl.num_programs(0) - 1)
     def _():
-        state = acc[...].astype(BF16)
+        load.wait()
+        rows = w_ref.shape[2]
+        for s in range(w_ref.shape[0]):
+            piece = jnp.zeros((tokens, rows), F32)
+            for u in range(w_ref.shape[1]):
+                piece += lax.dot_general(
+                    attended[u], w_ref[s, u], (((1,), (1,)), ((), ())), preferred_element_type=F32
+                )
+            where = slice(s * rows, (s + 1) * rows)
+            if last:
+                acc[:, where] = piece.astype(BF16)
+            else:
+                out_ref[:, where] = piece.astype(BF16)
         if last:
-            wide = state.astype(F32)
+            wide = acc[...].astype(F32)
             inv_root = lax.rsqrt(jnp.mean(wide * wide, axis=-1, keepdims=True) + EPS)
             out_ref[...] = wide * inv_root * gain_ref[...]
-        else:
-            out_ref[...] = state
 
 
 def gather_weights(packed):
@@ -130,6 +129,7 @@
         jnp.concatenate([query_weight, key_weight, value_weight, output_weight], axis=2)
     )
     sinks = lax.all_gather(sink_logit, "tp", axis=1, tiled=True)
+    whole, sinks = lax.optimization_barrier((whole, sinks))
 
     half = HEAD_DIM // 2
     inverse = 10000.0 ** (-jnp.arange(half).astype(F32) / half)
@@ -145,7 +145,12 @@
     one = jnp.ones((tokens, kv_cols), F32)
     cos_table = jnp.concatenate([jnp.tile(pair_c * root, (1, heads)), jnp.tile(pair_c, (1, groups)), one], axis=1)
     sin_table = jnp.concatenate([jnp.tile(pair_s * root, (1, heads)), jnp.tile(pair_s, (1, groups)), 0 * one], axis=1)
-    offset_row = jnp.reshape(offset, (1,)).astype(jnp.int32)
+    span = 3 * WINDOW
+    row = jnp.arange(tokens, dtype=jnp.int32)[:, None]
+    reach = jnp.arange(span, dtype=jnp.int32)[None, :] - WINDOW
+    key_pos = offset + row - row % WINDOW + reach
+    allowed = (jnp.abs(row % WINDOW - reach) <= WINDOW) & (key_pos >= 0) & (key_pos < seq_total)
+    bias = jnp.where(allowed, 0.0, -jnp.inf).astype(F32)
 
     count = n_sp * n_tp
     forward = [(i, i + 1) for i in range(count - 1)]
@@ -174,24 +179,29 @@
         low = lax.ppermute(kv[:, tokens - WINDOW :], AXES, forward)
         high = lax.ppermute(kv[:, :WINDOW], AXES, backward)
         current = pl.pallas_call(
-            functools.partial(attend_kernel, layer, last, seq_total),
+            functools.partial(attend_kernel, layer, last),
             name="attend",
             grid=(n_tp,),
             out_shape=jax.ShapeDtypeStruct((tokens, features), F32 if last else BF16),
             in_specs=[
                 smem,
-                smem,
                 pl.BlockSpec((1, tokens, cols), lambda t: (t, 0, 0)),
                 pl.BlockSpec((1, tokens, cols), lambda t: (t, 0, 0)),
                 pl.BlockSpec((1, WINDOW, cols), lambda t: (t, 0, 0)),
                 pl.BlockSpec((1, WINDOW, cols), lambda t: (t, 0, 0)),
-                pl.BlockSpec((n_sp, 1, 1, rows, cols), lambda t, l=layer: (0, t, l, 0, 2)),
+                full(tokens, span),
+                pl.BlockSpec(memory_space=pl.ANY),
                 full(1, features),
             ],
             out_specs=full(tokens, features),
-            scratch_shapes=[pltpu.VMEM((tokens, features), F32)],
+            scratch_shapes=[
+                pltpu.VMEM((n_sp, n_tp, rows, cols), BF16),
+                pltpu.VMEM((n_tp, tokens, cols), BF16),
+                pltpu.VMEM((tokens, features), BF16),
+                pltpu.SemaphoreType.DMA,
+            ],
             compiler_params=pltpu.CompilerParams(vmem_limit_bytes=VMEM_LIMIT),
-        )(sinks, offset_row, queries, kv, low, high, whole, final_gain[None])
+        )(sinks, queries, kv, low, high, bias, whole, final_gain[None])
     return current
 
 

time: 345 us -> 315 us (0.913)
  Pallas kernels: 74.9 us -> 45.7 us
    pallas_call x3, Pallas kernels: 54.4 us -> 25.3 us  [shards(): pl.pallas_call(functools.partial(attend_kernel, layer, last), name='atten...]
    all_gather x1, waiting for transfers between devices: 213 us -> 207 us  [gather_weights(): whole = lax.all_gather(packed, AXES, axis=0, tiled=False)]
    ppermute x3, waiting for transfers between devices: 13 us -> 16.8 us  [shards(): low = lax.ppermute(kv[:, tokens - WINDOW:], AXES, forward)]
  transfers between devices with their start and end apart: 7 -> 7, of which waited for: 6 -> 7; matrix products, arithmetic and copies ran while one was open for 1% -> 1% of each run, Pallas kernels for 0% -> 0%
where the time goes in v2:
time: 315 us; the launch traced here: 314 us
  waiting for transfers between devices  229 us (73%)
  Pallas kernels  45.7 us (15%)
  starting transfers between devices  15.8 us (5%)
  between operations  13.7 us (4%)
  blocking collectives  5.18 us (2%)
    all_gather x1, waiting for transfers between devices, gather_weights(): whole = lax.all_gather(packed, AXES, axis=0, tiled=False)  207 us
    pallas_call x3, Pallas kernels, shards(): pl.pallas_call(functools.partial(attend_kernel, layer, last), name='atten...  25.3 us
    pallas_call x3, Pallas kernels, shards(): pl.pallas_call(project_kernel, name='project', grid=(n_tp,), out_shape=[j...  20.4 us
    ppermute x3, waiting for transfers between devices, shards(): low = lax.ppermute(kv[:, tokens - WINDOW:], AXES, forward)  16.8 us
    ppermute x3, starting transfers between devices, shards(): high = lax.ppermute(kv[:, :WINDOW], AXES, backward)  8.91 us
    ppermute x3, starting transfers between devices, shards(): low = lax.ppermute(kv[:, tokens - WINDOW:], AXES, forward)  6.91 us
  transfers between devices with their start and end apart: 7, of which 7 were waited for; matrix products, arithmetic and copies ran while one was open for 1% of the time, Pallas kernels for 0%

profile of v2, /device:TPU:8, one launch (start us, length us, event | category | flops | bytes accessed | tf_op | source)
XLA Modules:
  0.0 314.1 jit_solution(6567806902425213224)
XLA Ops:
  6.5 0.0 copy-start.2
  6.5 0.0 all-gather.4.cloned.1.call-start
  6.5 2.4 pad_maximum_fusion
  8.9 0.0 all-gather.4.cloned.1.call-update
  9.0 0.0 copy-done.2
  9.0 0.1 copy.17
  9.1 5.2 %all-gather.1 = f32[4,4,3]{2,1,0:T(4,128)S(1)} all-gather(f32[1,4,3]{2,1,0:T(4,128)S(1)} %bitcast.27), channel_id=1, replica_groups=mesh['sp'=8,'tp'=4] {'tp'}, dimensions={0}, use_global_device_ids=true | all-gather | bytes 240 | tf_op jit(solution)/shard_map/all_gather | solution.py:131
  14.3 0.1 copy.23
  14.4 0.2 fusion.7
  14.6 0.1 copy.20
  14.8 0.1 copy.22
  14.9 0.1 copy.19
  15.0 0.0 copy-start.1
  15.1 0.1 copy.21
  15.2 0.1 maximum_maximum_fusion.cos_ref
  15.3 0.1 maximum_maximum_fusion.1.sin_ref
  15.3 1.3 constant_dynamic-slice_fusion.cur_ref
  16.6 0.0 copy-done.1
  16.7 207.2 %all-gather.4.cloned.1.call-done = bf16[96,256,768]{2,1,0:T(8,128)(2,1)} async-done(((bf16[3,256,768]{2,1,0:T(8,128)(2,1)}), bf16[96,256,768]{2,1,0:T(8,128)(2,1)}) %all-gather.4.cloned.1.call-update) | async-done | bytes 37748752 | tf_op jit(solution)/shard_map/all_gather | solution.py:113
  223.9 0.0 copy-start
  223.9 6.8 %project.3 = (bf16[4,256,256]{2,1,0:T(8,128)(2,1)S(1)}, bf16[4,256,256]{2,1,0:T(8,128)(2,1)S(1)}) custom-call(bf16[256,2048]{1,0:T(8,128)(2,1)S(1)} %constant_dynamic-slice_fusion.cur_ref, f32[1,2048]{1,0:T(1,128)S(1)} %get-tuple-element.30.gain_ref, bf16[8,4,3,256,768]{4,3,2,1,0:T(8,128)(2,1)} %bitcast.16, f32[256,512]{1,0:T(8,128)S(1)} %maximum_maximum_fusion.cos_ref, ...), custom_call_target="tpu_custom_call" | custom-call | tf_op jit(solution)/shard_map/project/pallas_call | solution.py:163
  230.8 5.1 %collective-permute-start.1 = (bf16[4,128,256]{2,1,0:T(8,128)(2,1)S(1)}, bf16[4,128,256]{2,1,0:T(8,128)(2,1)S(1)}, u32[]{:S(2)}, u32[]{:S(2)}) collective-permute-start(bf16[4,128,256]{2,1,0:T(8,128)(2,1)S(1)} %get-tuple-element.25), channel_id=1, source_target_pairs={{1,0},{2,1},{3,2},{4,3},{5,4},{6,5},{7,6},{8,7},{9,8},{10,9},{11,1... | collective-permute-start | bytes 786440 | tf_op jit(solution)/shard_map/ppermute | solution.py:180
  235.9 1.9 collective-permute-start
  237.8 0.2 fusion.2.bias_ref
  238.0 1.7 collective-permute-done.1.hi_ref
  239.8 5.6 %collective-permute-done.lo_ref = bf16[4,128,256]{2,1,0:T(8,128)(2,1)S(1)} collective-permute-done((bf16[4,128,256]{2,1,0:T(8,128)(2,1)S(1)}, bf16[4,128,256]{2,1,0:T(8,128)(2,1)S(1)}, u32[]{:S(2)}, u32[]{:S(2)}) %collective-permute-start) | collective-permute-done | bytes 262176 | tf_op jit(solution)/shard_map/ppermute | solution.py:179
  245.4 0.0 copy-done
  245.4 7.9 %attend.3.cur_ref = bf16[256,2048]{1,0:T(8,128)(2,1)S(1)} custom-call(f32[3,16]{1,0:T(4,128)S(1)} %bitcast.13, bf16[4,256,256]{2,1,0:T(8,128)(2,1)S(1)} %get-tuple-element.15.q_ref, bf16[4,256,256]{2,1,0:T(8,128)(2,1)S(1)} %get-tuple-element.16.kv_ref, bf16[4,128,256]{2,1,0:T(8,128)(2,1)S(1)} %collective-permute-done.lo_ref, ...), custom_call_target="tpu_custom_call" | custom-call | tf_op jit(solution)/shard_map/attend/pallas_call | solution.py:181
  253.3 6.8 %project.4 = (bf16[4,256,256]{2,1,0:T(8,128)(2,1)S(1)}, bf16[4,256,256]{2,1,0:T(8,128)(2,1)S(1)}) custom-call(bf16[256,2048]{1,0:T(8,128)(2,1)S(1)} %attend.3.cur_ref, f32[1,2048]{1,0:T(1,128)S(1)} %get-tuple-element.31.gain_ref, bf16[8,4,3,256,768]{4,3,2,1,0:T(8,128)(2,1)} %bitcast.18, f32[256,512]{1,0:T(8,128)S(1)} %maximum_maximum_fusion.cos_ref, ...), custom_call_target="tpu_custom_call" | custom-call | tf_op jit(solution)/shard_map/project/pallas_call | solution.py:163
  260.2 1.9 collective-permute-start.3
  262.1 2.4 collective-permute-start.2
  264.5 1.5 collective-permute-done.3.hi_ref
  266.0 5.6 %collective-permute-done.2.lo_ref = bf16[4,128,256]{2,1,0:T(8,128)(2,1)S(1)} collective-permute-done((bf16[4,128,256]{2,1,0:T(8,128)(2,1)S(1)}, bf16[4,128,256]{2,1,0:T(8,128)(2,1)S(1)}, u32[]{:S(2)}, u32[]{:S(2)}) %collective-permute-start.2) | collective-permute-done | bytes 262176 | tf_op jit(solution)/shard_map/ppermute | solution.py:179
  271.6 7.9 %attend.4.cur_ref = bf16[256,2048]{1,0:T(8,128)(2,1)S(1)} custom-call(f32[3,16]{1,0:T(4,128)S(1)} %bitcast.14, bf16[4,256,256]{2,1,0:T(8,128)(2,1)S(1)} %get-tuple-element.17.q_ref, bf16[4,256,256]{2,1,0:T(8,128)(2,1)S(1)} %get-tuple-element.18.kv_ref, bf16[4,128,256]{2,1,0:T(8,128)(2,1)S(1)} %collective-permute-done.2.lo_ref, ...), custom_call_target="tpu_custom_call" | custom-call | tf_op jit(solution)/shard_map/attend/pallas_call | solution.py:181
  279.5 6.8 %project.5 = (bf16[4,256,256]{2,1,0:T(8,128)(2,1)S(1)}, bf16[4,256,256]{2,1,0:T(8,128)(2,1)S(1)}) custom-call(bf16[256,2048]{1,0:T(8,128)(2,1)S(1)} %attend.4.cur_ref, f32[1,2048]{1,0:T(1,128)S(1)} %get-tuple-element.29.gain_ref, bf16[8,4,3,256,768]{4,3,2,1,0:T(8,128)(2,1)} %bitcast.20, f32[256,512]{1,0:T(8,128)S(1)} %maximum_maximum_fusion.cos_ref, ...), custom_call_target="tpu_custom_call" | custom-call | tf_op jit(solution)/shard_map/project/pallas_call | solution.py:163
  286.4 1.9 collective-permute-start.5
  288.3 2.6 collective-permute-start.4
  290.9 1.3 collective-permute-done.5.hi_ref
  292.2 5.6 %collective-permute-done.4.lo_ref = bf16[4,128,256]{2,1,0:T(8,128)(2,1)S(1)} collective-permute-done((bf16[4,128,256]{2,1,0:T(8,128)(2,1)S(1)}, bf16[4,128,256]{2,1,0:T(8,128)(2,1)S(1)}, u32[]{:S(2)}, u32[]{:S(2)}) %collective-permute-start.4) | collective-permute-done | bytes 262176 | tf_op jit(solution)/shard_map/ppermute | solution.py:179
  297.8 9.4 %attend.5 = f32[256,2048]{1,0:T(8,128)} custom-call(f32[3,16]{1,0:T(4,128)S(1)} %bitcast.15, bf16[4,256,256]{2,1,0:T(8,128)(2,1)S(1)} %get-tuple-element.19.q_ref, bf16[4,256,256]{2,1,0:T(8,128)(2,1)S(1)} %get-tuple-element.20.kv_ref, bf16[4,128,256]{2,1,0:T(8,128)(2,1)S(1)} %collective-permute-done.4.lo_ref, ...), custom_call_target="tpu_custom_call" | custom-call | tf_op jit(solution)/shard_map/attend/pallas_call | solution.py:181
  (17 shorter events, 0.3 us)
Async XLA Ops:
  6.5 2.5 copy-start.2
  6.5 217.4 %all-gather.4.cloned.1.call-start = ((), (), s32[]{:S(2)}) async-start(), calls=%async_computation | async-start | bytes 38928384 | tf_op jit(solution)/shard_map/all_gather | solution.py:113
  15.0 1.6 copy-start.1
  223.9 21.4 %copy-start = (f32[2048]{0:T(1024)S(1)}, f32[2048]{0:T(1024)}, u32[]{:S(2)}) copy-start(f32[2048]{0:T(1024)} %param.15) | copy-start | bytes 24580
  230.8 9.0 %collective-permute-start.1 = (bf16[4,128,256]{2,1,0:T(8,128)(2,1)S(1)}, bf16[4,128,256]{2,1,0:T(8,128)(2,1)S(1)}, u32[]{:S(2)}, u32[]{:S(2)}) collective-permute-start(bf16[4,128,256]{2,1,0:T(8,128)(2,1)S(1)} %get-tuple-element.25), channel_id=1, source_target_pairs={{1,0},{2,1},{3,2},{4,3},{5,4},{6,5},{7,6},{8,7},{9,8},{10,9},{11,1... | collective-permute-start | bytes 786440 | tf_op jit(solution)/shard_map/ppermute | solution.py:180
  235.9 9.5 %collective-permute-start = (bf16[4,128,256]{2,1,0:T(8,128)(2,1)S(1)}, bf16[4,128,256]{2,1,0:T(8,128)(2,1)S(1)}, u32[]{:S(2)}, u32[]{:S(2)}) collective-permute-start(bf16[4,128,256]{2,1,0:T(8,128)(2,1)S(1)} %get-tuple-element.26), channel_id=1, source_target_pairs={{0,1},{1,2},{2,3},{3,4},{4,5},{5,6},{6,7},{7,8},{8,9},{9,10},{10,1... | collective-permute-start | bytes 786440 | tf_op jit(solution)/shard_map/ppermute | solution.py:179
  260.2 5.8 %collective-permute-start.3 = (bf16[4,128,256]{2,1,0:T(8,128)(2,1)S(1)}, bf16[4,128,256]{2,1,0:T(8,128)(2,1)S(1)}, u32[]{:S(2)}, u32[]{:S(2)}) collective-permute-start(bf16[4,128,256]{2,1,0:T(8,128)(2,1)S(1)} %get-tuple-element.23), channel_id=1, source_target_pairs={{1,0},{2,1},{3,2},{4,3},{5,4},{6,5},{7,6},{8,7},{9,8},{10,9},{11,1... | collective-permute-start | bytes 786440 | tf_op jit(solution)/shard_map/ppermute | solution.py:180
  262.1 9.5 %collective-permute-start.2 = (bf16[4,128,256]{2,1,0:T(8,128)(2,1)S(1)}, bf16[4,128,256]{2,1,0:T(8,128)(2,1)S(1)}, u32[]{:S(2)}, u32[]{:S(2)}) collective-permute-start(bf16[4,128,256]{2,1,0:T(8,128)(2,1)S(1)} %get-tuple-element.24), channel_id=1, source_target_pairs={{0,1},{1,2},{2,3},{3,4},{4,5},{5,6},{6,7},{7,8},{8,9},{9,10},{10,1... | collective-permute-start | bytes 786440 | tf_op jit(solution)/shard_map/ppermute | solution.py:179
  286.4 5.8 %collective-permute-start.5 = (bf16[4,128,256]{2,1,0:T(8,128)(2,1)S(1)}, bf16[4,128,256]{2,1,0:T(8,128)(2,1)S(1)}, u32[]{:S(2)}, u32[]{:S(2)}) collective-permute-start(bf16[4,128,256]{2,1,0:T(8,128)(2,1)S(1)} %get-tuple-element.21), channel_id=1, source_target_pairs={{1,0},{2,1},{3,2},{4,3},{5,4},{6,5},{7,6},{8,7},{9,8},{10,9},{11,1... | collective-permute-start | bytes 786440 | tf_op jit(solution)/shard_map/ppermute | solution.py:180
  288.3 9.5 %collective-permute-start.4 = (bf16[4,128,256]{2,1,0:T(8,128)(2,1)S(1)}, bf16[4,128,256]{2,1,0:T(8,128)(2,1)S(1)}, u32[]{:S(2)}, u32[]{:S(2)}) collective-permute-start(bf16[4,128,256]{2,1,0:T(8,128)(2,1)S(1)} %get-tuple-element.22), channel_id=1, source_target_pairs={{0,1},{1,2},{2,3},{3,4},{4,5},{5,6},{6,7},{7,8},{8,9},{9,10},{10,1... | collective-permute-start | bytes 786440 | tf_op jit(solution)/shard_map/ppermute | solution.py:179
Sparse Core Ops, SparseCore 0:
  10.2 213.6 all-gather.3
